TPU v7x, 512 devices: a whole 4x8x8 slice. The times are simulated.
512 devices in a mesh: sp: 64 (over z, y), tp: 8 (over x, core).
Axes of the slice: x: 4, y: 8, z: 8, core: 2. Of those that a mesh axis runs over, the one named last changes fastest.
Arguments:
- residual: bfloat16 [8192, 2048], P('sp', 'tp'), may hold values from -24 to 24
- queries: bfloat16 [8192, 2048], P('sp', 'tp'), may hold values from -16 to 16
- key_proj: bfloat16 [8192, 512], P(('sp', 'tp')), may hold values from -8 to 8
- value_proj: bfloat16 [8192, 512], P(('sp', 'tp')), may hold values from -6 to 6
- diff_lambda: float32 [8], replicated, may hold values from 0.3 to 0.8
- head_gain: float32 [256], replicated, may hold values from 0.1 to 1.9
- out_weight: bfloat16 [2048, 2048], P(None, 'tp'), may hold values from -0.125 to 0.125
- norm_gain: float32 [2048], P('tp'), may hold values from 0.1 to 1.9
- up_weight: bfloat16 [2048, 8192], P('sp', 'tp'), may hold values from -0.125 to 0.125
- down_weight: bfloat16 [8192, 2048], P('tp', 'sp'), may hold values from -0.0625 to 0.0625
Outputs:
- layer_out: bfloat16 [8192, 2048], P('sp', 'tp')
All inputs are finite; a program needn't handle non-finite values.
Results may differ from a plain program's by a relative error of at most 0.012.
Values may be sent and summed in bfloat16 or wider, within the bound.
A program may use at most 64 MiB of HBM per device.

v0:
```python
import jax
import jax.numpy as jnp
from jax import lax
from jax.sharding import PartitionSpec as P

D = 2048
HEADS = 8
KV_HEADS = 2
HEAD_DIM = 128
VALUE_DIM = 256
epsilon = 1e-06


def turned_gather(arrays, axis, dims):
    turned = [jnp.moveaxis(a, dim, 0) for a, dim in zip(arrays, dims)]
    both = jnp.concatenate([t.reshape(len(t), -1) for t in turned], axis=1)
    whole, at, finished = (lax.all_gather(both, axis, axis=0, tiled=True), 0, [])
    for t, dim in zip(turned, dims):
        share = whole[:, at : at + t[0].size].reshape(-1, *t.shape[1:])
        finished.append(jnp.moveaxis(share, 0, dim))
        at += t[0].size
    return tuple(finished)


def from_everyone(shard, axis):
    copies = jnp.broadcast_to(shard, (lax.axis_size(axis), *shard.shape))
    return lax.all_to_all(copies, axis, split_axis=0, concat_axis=0, tiled=True)


def laid_out(parts, dim):
    dims = list(parts.shape[1:])
    dims[dim] *= parts.shape[0]
    return jnp.moveaxis(parts, 0, dim).reshape(dims)


def collect(shard, axis, dim):
    parts = from_everyone(shard, axis)
    return laid_out(parts, dim)


def sent_together(arrays, axis, dim, along):
    ends, at = ([], 0)
    for a in arrays[:-1]:
        at += a.shape[along]
        ends.append(at)
    both = jnp.concatenate(arrays, axis=along)
    return tuple(jnp.split(lax.all_gather(both, axis, axis=dim, tiled=True), ends, axis=along))


def side_by_side(arrays, axis, split_dim, concat_dim, along):
    columns = [a.reshape(*a.shape[:along], -1) for a in arrays]
    both = jnp.concatenate(columns, axis=along)
    whole, at, finished = (
        lax.all_to_all(both, axis, split_axis=split_dim, concat_axis=concat_dim, tiled=True),
        0,
        [],
    )
    for a, column in zip(arrays, columns):
        share = whole[..., at : at + column.shape[along]]
        finished.append(share.reshape(*share.shape[:along], *a.shape[along:]))
        at += column.shape[along]
    return tuple(finished)


def over_copies(shard, axis):
    everything = from_everyone(shard, axis)
    return jnp.sum(everything, axis=0)


def split_up(shard, dim, length):
    dims = shard.shape
    parts = shard.reshape(*dims[:dim], length, dims[dim] // length, *dims[dim + 1 :])
    return jnp.moveaxis(parts, dim, 0)


def sent_and_summed(shard, axis, dim):
    parts = split_up(shard, dim, lax.axis_size(axis))
    arrived = lax.all_to_all(parts, axis, split_axis=0, concat_axis=0, tiled=True)
    return arrived.sum(axis=0)


def head_norm(per_map, lambdas, gain):
    difference = per_map[:, 0] - lambdas[:, None, None] * per_map[:, 1]
    scaled = (
        difference
        * lax.rsqrt(jnp.mean(difference * difference, axis=-1, keepdims=True) + epsilon)
        * gain
    )
    return scaled.astype(jnp.bfloat16)


def on_device(
    residual,
    queries,
    key_proj,
    value_proj,
    diff_lambda,
    head_gain,
    out_weight,
    norm_gain,
    up_weight,
    down_weight,
):
    up_whole, down_whole = turned_gather((up_weight, down_weight), "sp", (0, 1))
    rows_here = residual.shape[0]
    per_group = HEADS // KV_HEADS
    scaling = HEAD_DIM ** (-0.5)
    all_queries = collect(queries, "tp", 1)
    query_grid = all_queries.reshape(rows_here, KV_HEADS, per_group, 2, HEAD_DIM)
    stat_shape = (KV_HEADS, per_group, 2, rows_here)
    maxima = jnp.full(stat_shape, -1e30, jnp.float32)
    key_piece, value_piece = sent_together((key_proj, value_proj), "sp", 0, 1)
    key_count = key_piece.shape[0]
    key_grid = key_piece.reshape(key_count, KV_HEADS, 2, HEAD_DIM)
    value_grid = value_piece.reshape(key_count, KV_HEADS, VALUE_DIM)
    scores = (
        jnp.einsum("qagcd,kacd->agcqk", query_grid, key_grid, preferred_element_type=jnp.float32)
        * scaling
    )
    highest = jnp.maximum(maxima, jnp.max(scores, axis=-1))
    weights = jnp.exp(scores - highest[..., None])
    totals = jnp.sum(weights, axis=-1)
    weighted = jnp.einsum(
        "agcqk,kae->agcqe",
        weights.astype(jnp.bfloat16),
        value_grid,
        preferred_element_type=jnp.float32,
    )
    maxima, totals, weighted = (highest, totals, weighted)
    maxima = maxima.reshape(HEADS, 2, rows_here)
    totals = totals.reshape(HEADS, 2, rows_here)
    weighted = weighted.reshape(HEADS, 2, rows_here, VALUE_DIM)
    tp_size = lax.axis_size("tp")
    local_heads = HEADS // tp_size
    got_max, got_tot, got_sum = side_by_side((maxima, totals, weighted), "tp", 0, 0, 3)
    got_max = got_max.reshape(tp_size, local_heads, 2, rows_here)
    got_tot = got_tot.reshape(tp_size, local_heads, 2, rows_here)
    got_sum = got_sum.reshape(tp_size, local_heads, 2, rows_here, VALUE_DIM)
    highest = jnp.max(got_max, axis=0)
    factor = jnp.exp(got_max - highest)
    totals_all = jnp.sum(factor * got_tot, axis=0)
    sums_all = jnp.sum(factor[..., None] * got_sum, axis=0)
    lambdas = lax.dynamic_slice_in_dim(diff_lambda, lax.axis_index("tp") * local_heads, local_heads)
    own_heads = head_norm(sums_all / totals_all[..., None], lambdas, head_gain)
    head_outputs = collect(own_heads, "tp", 0)
    out_grid = out_weight.reshape(HEADS, VALUE_DIM, out_weight.shape[1])
    projected = jnp.einsum(
        "hqe,hed->qd", head_outputs, out_grid, preferred_element_type=jnp.float32
    )
    after_mix = residual.astype(jnp.float32) + projected
    squares = over_copies(jnp.sum(after_mix * after_mix, axis=1), "tp")
    normed = (after_mix * lax.rsqrt(squares / D + epsilon)[:, None] * norm_gain).astype(
        jnp.bfloat16
    )
    full_rows = collect(normed, "tp", 1)
    hidden = jnp.dot(full_rows, up_whole, preferred_element_type=jnp.float32)
    activated = jnp.square(jax.nn.relu(hidden)).astype(jnp.bfloat16)
    partial_value = jnp.dot(activated, down_whole, preferred_element_type=jnp.float32)
    mixer_sum = sent_and_summed(partial_value, "tp", 1)
    return (after_mix + mixer_sum).astype(jnp.bfloat16)


def solution(mesh):
    return jax.shard_map(
        on_device,
        mesh=mesh,
        in_specs=(
            P("sp", "tp"),
            P("sp", "tp"),
            P(("sp", "tp"), None),
            P(("sp", "tp"), None),
            P(),
            P(),
            P(None, "tp"),
            P("tp"),
            P("sp", "tp"),
            P("tp", "sp"),
        ),
        out_specs=P("sp", "tp"),
        check_vma=False,
    )
```

profile of v0, /device:TPU:1, one launch (start us, length us, event | category | flops | bytes accessed | tf_op | source)
XLA Modules:
  0.0 231.3 jit_solution(17370695818168791017)
XLA Ops:
  6.5 1.4 pad_maximum_fusion.2
  8.1 1.5 pad_maximum_fusion.1
  9.6 1.0 copy.62
  10.6 0.9 broadcast_in_dim.10
  11.4 10.9 %all-to-all-start = ((bf16[8,128,256]{1,2,0:T(8,128)(2,1)}), bf16[8,128,256]{1,2,0:T(8,128)(2,1)}, u32[]{:S(2)}, u32[]{:S(2)}) async-start(bf16[8,128,256]{1,2,0:T(8,128)(2,1)} %broadcast_in_dim.10), calls=%async_computation | async-start | bytes 1048576 | tf_op jit(solution)/shard_map/all_to_all | solution.py:27
  22.3 72.8 %all-gather.3.cloned.1.call-done = bf16[1024,1024]{1,0:T(8,128)(2,1)} async-done(((bf16[16,1024]{1,0:T(8,128)(2,1)}), bf16[1024,1024]{1,0:T(8,128)(2,1)}) %all-gather.3.cloned.1.call-update) | async-done | bytes 2097168 | tf_op jit(solution)/shard_map/all_gather | solution.py:47
  95.1 1.7 fusion.34
  96.8 1.4 copy.93
  98.7 2.3 %bitcast_reduce_fusion = (f32[2,4,2,128]{3,1,2,0:T(4,128)S(1)}, f32[2,2,1024,128,4]{3,2,4,1,0:T(8,128)S(1)}) fusion(bf16[1024,2,2,128,1]{0,3,4,2,1:T(8,128)(2,1)S(1)} %bitcast.73, bf16[128,2,4,2,128]{0,4,3,2,1:T(8,128)(2,1)} %bitcast.3), kind=kOutput, calls=%fused_computation.1 | convolution fusion | flops 541063168 | bytes 9969664 | tf_op jit(solution)/shard_map/qagcd,kacd->agcqk/dot_general | solution.py:117
  101.1 1.8 fusion.2
  102.9 3.2 %fusion.7 = f32[2,4,2,128,256]{4,3,2,1,0:T(8,128)} fusion(bf16[1024,2,256,1,1]{0,2,4,3,1:T(8,128)(2,1)S(1)} %bitcast.75, bf16[2,4,2,128,1024]{3,4,1,2,0:T(8,128)(2,1)S(1)} %get-tuple-element.8), kind=kOutput, calls=%fused_computation.9 | convolution fusion | flops 1073741824 | bytes 7340032 | tf_op jit(solution)/shard_map/agcqk,kae->agcqe/dot_general | solution.py:123
  106.0 2.8 %copy.72 = f32[8,2,128,256]{2,1,3,0:T(2,128)S(1)} copy(f32[8,2,128,256]{3,2,1,0:T(8,128)} %bitcast.74) | data formatting | bytes 4194304 | tf_op jit(solution)/shard_map/reshape | solution.py:132
  108.9 2.1 pad_maximum_fusion
  111.0 9.4 %all-to-all-start.1 = ((f32[8,2,128,258]{2,1,3,0:T(2,128)}), f32[8,2,128,258]{2,1,3,0:T(2,128)S(1)}, u32[]{:S(2)}, u32[]{:S(2)}) async-start(f32[8,2,128,258]{2,1,3,0:T(2,128)} %pad_maximum_fusion), calls=%async_computation.1 | async-start | bytes 4227072 | tf_op jit(solution)/shard_map/all_to_all | solution.py:54
  121.0 25.8 %all-to-all-done.1 = f32[8,2,128,258]{2,1,3,0:T(2,128)S(1)} async-done(((f32[8,2,128,258]{2,1,3,0:T(2,128)}), f32[8,2,128,258]{2,1,3,0:T(2,128)S(1)}, u32[]{:S(2)}, u32[]{:S(2)}) %all-to-all-start.1) | async-done | bytes 2113568 | tf_op jit(solution)/shard_map/all_to_all | solution.py:54
  146.9 1.0 fusion.9
  147.9 0.9 multiply_reduce_fusion.1
  149.2 12.8 %all_to_all.31 = bf16[8,1,128,256]{3,2,1,0:T(8,128)(2,1)S(1)} all-to-all(bf16[8,1,128,256]{3,2,1,0:T(8,128)(2,1)S(1)} %broadcast_in_dim.12), channel_id=1, replica_groups=mesh['sp'=64,'tp'=8] {'tp'}, dimensions={0} | all-to-all | bytes 1048576 | tf_op jit(solution)/shard_map/all_to_all | solution.py:27
  162.3 8.0 %all_to_all.32 = f32[8,1,128]{2,1,0:T(1,128)S(1)} all-to-all(f32[8,1,128]{2,1,0:T(1,128)S(1)} %broadcast_in_dim.13), channel_id=1, replica_groups=mesh['sp'=64,'tp'=8] {'tp'}, dimensions={0} | all-to-all | bytes 8192 | tf_op jit(solution)/shard_map/all_to_all | solution.py:27
  170.7 12.4 %all_to_all.33 = bf16[8,128,256]{1,2,0:T(8,128)(2,1)S(1)} all-to-all(bf16[8,128,256]{1,2,0:T(8,128)(2,1)S(1)} %broadcast_in_dim.28), channel_id=1, replica_groups=mesh['sp'=64,'tp'=8] {'tp'}, dimensions={0} | all-to-all | bytes 1048576 | tf_op jit(solution)/shard_map/all_to_all | solution.py:27
  183.1 15.0 %all-gather.5.cloned.1.call-done = bf16[2048,2048]{1,0:T(8,128)(2,1)} async-done(((bf16[32,2048]{1,0:T(8,128)(2,1)}), bf16[2048,2048]{1,0:T(8,128)(2,1)}) %all-gather.5.cloned.1.call-update) | async-done | bytes 8388624 | tf_op jit(solution)/shard_map/all_gather | solution.py:17
  198.1 5.6 %fusion.3 = f32[128,2048]{1,0:T(8,128)S(1)} fusion(bf16[2048,2048]{1,0:T(8,128)(2,1)} %all-gather.5.cloned.1.call-done, bf16[128,2048]{0,1:T(8,128)(2,1)S(1)} %bitcast.78), kind=kOutput, calls=%fused_computation.5 | convolution fusion | flops 1074135040 | bytes 9961472 | tf_op jit(solution)/shard_map/dot_general | solution.py:158
  203.8 19.9 %all_to_all.34 = f32[8,128,256]{2,1,0:T(8,128)S(1)} all-to-all(f32[8,128,256]{2,1,0:T(8,128)S(1)} %bitcast.72), channel_id=1, replica_groups=mesh['sp'=64,'tp'=8] {'tp'}, dimensions={0} | all-to-all | bytes 2097152 | tf_op jit(solution)/shard_map/all_to_all | solution.py:78
  223.8 0.6 add_convert_fusion
  (42 shorter events, 2.5 us)
Async XLA Ops:
  6.5 155.4 %copy-start = (bf16[2048,256]{1,0:T(8,128)(2,1)S(1)}, bf16[2048,256]{1,0:T(8,128)(2,1)}, u32[]{:S(2)}) copy-start(bf16[2048,256]{1,0:T(8,128)(2,1)} %param.16) | copy-start | bytes 3145732
  6.5 88.5 %all-gather.3.cloned.1.call-start = ((), (), s32[]{:S(2)}) async-start(), calls=%async_computation.6 | async-start | bytes 2129920 | tf_op jit(solution)/shard_map/all_gather | solution.py:47
  8.0 190.1 %all-gather.5.cloned.1.call-start = ((), (), s32[]{:S(2)}) async-start(), calls=%async_computation.7 | async-start | bytes 8519680 | tf_op jit(solution)/shard_map/all_gather | solution.py:17
  11.4 87.2 %all-to-all-start = ((bf16[8,128,256]{1,2,0:T(8,128)(2,1)}), bf16[8,128,256]{1,2,0:T(8,128)(2,1)}, u32[]{:S(2)}, u32[]{:S(2)}) async-start(bf16[8,128,256]{1,2,0:T(8,128)(2,1)} %broadcast_in_dim.10), calls=%async_computation | async-start | bytes 1048576 | tf_op jit(solution)/shard_map/all_to_all | solution.py:27
  101.1 1.8 copy-start.1
  108.9 11.5 %copy-start.5 = (f32[8]{0:T(128)S(1)}, f32[8]{0:T(128)}, u32[]{:S(2)}) copy-start(f32[8]{0:T(128)} %param.14) | copy-start | bytes 100
  111.0 37.9 %copy-start.3 = (f32[256]{0:T(256)S(1)}, f32[256]{0:T(256)}, u32[]{:S(2)}) copy-start(f32[256]{0:T(256)} %param.15) | copy-start | bytes 3076
  111.0 50.9 %copy-start.2 = (bf16[128,256]{1,0:T(8,128)(2,1)S(1)}, bf16[128,256]{1,0:T(8,128)(2,1)}, u32[]{:S(2)}) copy-start(bf16[128,256]{1,0:T(8,128)(2,1)} %param.10) | copy-start | bytes 196612
  111.0 35.8 %all-to-all-start.1 = ((f32[8,2,128,258]{2,1,3,0:T(2,128)}), f32[8,2,128,258]{2,1,3,0:T(2,128)S(1)}, u32[]{:S(2)}, u32[]{:S(2)}) async-start(f32[8,2,128,258]{2,1,3,0:T(2,128)} %pad_maximum_fusion), calls=%async_computation.1 | async-start | bytes 4227072 | tf_op jit(solution)/shard_map/all_to_all | solution.py:54
  120.4 50.0 %copy-start.4 = (f32[256]{0:T(256)S(1)}, f32[256]{0:T(256)}, u32[]{:S(2)}) copy-start(f32[256]{0:T(256)} %param.17) | copy-start | bytes 3076
Sparse Core Ops, SparseCore 0:
  10.4 84.6 all-gather.2
  98.1 99.9 all-gather.4
where the time goes:
time: 232 us; the launch traced here: 231 us
  waiting for transfers between devices  114 us (49%)
  blocking collectives  53.1 us (23%)
  starting transfers between devices  20.3 us (9%)
  between operations  13.6 us (6%)
  matrix products  11.5 us (5%)
  other arithmetic  9.83 us (4%)
  local copies, waits for them, and re-layouts  9.31 us (4%)
    all_gather x1, waiting for transfers between devices, sent_together(): lax.all_gather(both, axis, axis=dim, tiled=True)  72.8 us
    all_to_all x3, blocking collectives, from_everyone(): return lax.all_to_all(copies, axis, split_axis=0, concat_axis=0, tiled=True)  33.2 us
    all_to_all x1, waiting for transfers between devices, side_by_side(): lax.all_to_all(both, axis, split_axis=split_dim, concat_axis=concat_dim,...  25.8 us
    all_to_all x1, blocking collectives, sent_and_summed(): lax.all_to_all(parts, axis, split_axis=0, concat_axis=0, tiled=True)  19.9 us
    all_gather x1, waiting for transfers between devices, turned_gather(): lax.all_gather(both, axis, axis=0, tiled=True)  15 us
    all_to_all x1, starting transfers between devices, from_everyone(): return lax.all_to_all(copies, axis, split_axis=0, concat_axis=0, tiled=True)  10.9 us
    all_to_all x1, starting transfers between devices, side_by_side(): lax.all_to_all(both, axis, split_axis=split_dim, concat_axis=concat_dim,...  9.39 us
    dot_general x1, matrix products, on_device(): jnp.dot(activated, down_whole, preferred_element_type=jnp.float32)  5.59 us
  transfers between devices with their start and end apart: 4, of which 3 were waited for; matrix products, arithmetic and copies ran while one was open for 10% of the time, Pallas kernels for 0%

commit v1 on v0

--- a/solution.py
+++ b/solution.py
@@ -14,7 +14,13 @@
 def turned_gather(arrays, axis, dims):
     turned = [jnp.moveaxis(a, dim, 0) for a, dim in zip(arrays, dims)]
     both = jnp.concatenate([t.reshape(len(t), -1) for t in turned], axis=1)
-    whole, at, finished = (lax.all_gather(both, axis, axis=0, tiled=True), 0, [])
+    whole, at, finished = (
+        jnp.concatenate(
+            lax.all_to_all(jnp.stack([both] * lax.axis_size(axis)), axis, 0, 0), axis=0
+        ),
+        0,
+        [],
+    )
     for t, dim in zip(turned, dims):
         share = whole[:, at : at + t[0].size].reshape(-1, *t.shape[1:])
         finished.append(jnp.moveaxis(share, 0, dim))

time: 232 us -> 427 us (1.84)
  the two profiles are of different devices: /device:TPU:1 before, /device:TPU:24 now
where the time goes in v1:
time: 427 us
  blocking collectives  249 us (58%)
  waiting for transfers between devices  121 us (28%)
  between operations  13.7 us (3%)
  starting transfers between devices  12.2 us (3%)
  matrix products  11.4 us (3%)
  local copies, waits for them, and re-layouts  11.1 us (3%)
  other arithmetic  8.35 us (2%)
    all_to_all x1, blocking collectives, turned_gather(): lax.all_to_all(jnp.stack([both] * lax.axis_size(axis)), axis, 0, 0)  210 us
    all_gather x1, waiting for transfers between devices, sent_together(): lax.all_gather(both, axis, axis=dim, tiled=True)  83.9 us
    all_to_all x1, waiting for transfers between devices, side_by_side(): lax.all_to_all(both, axis, split_axis=split_dim, concat_axis=concat_dim,...  26.7 us
    all_to_all x2, blocking collectives, from_everyone(): return lax.all_to_all(copies, axis, split_axis=0, concat_axis=0, tiled=True)  20.4 us
    all_to_all x1, blocking collectives, sent_and_summed(): lax.all_to_all(parts, axis, split_axis=0, concat_axis=0, tiled=True)  18.4 us
    all_to_all x2, waiting for transfers between devices, from_everyone(): return lax.all_to_all(copies, axis, split_axis=0, concat_axis=0, tiled=True)  10.2 us
  transfers between devices with their start and end apart: 4, of which 3 were waited for; matrix products, arithmetic and copies ran while one was open for 1% of the time, Pallas kernels for 0%

profile of v1, /device:TPU:24, one launch (start us, length us, event | category | flops | bytes accessed | tf_op | source)
XLA Modules:
  0.0 426.6 jit_solution(12663066150266105149)
XLA Ops:
  6.5 1.4 pad_maximum_fusion.2
  8.0 1.0 copy.62
  9.0 0.9 broadcast_in_dim.10
  9.8 4.3 %all-to-all-start = ((bf16[8,128,256]{1,2,0:T(8,128)(2,1)}), bf16[8,128,256]{1,2,0:T(8,128)(2,1)}, u32[]{:S(2)}, u32[]{:S(2)}) async-start(bf16[8,128,256]{1,2,0:T(8,128)(2,1)} %broadcast_in_dim.10), calls=%async_computation | async-start | bytes 1048576 | tf_op jit(solution)/shard_map/all_to_all | solution.py:33
  14.1 83.9 %all-gather.2.cloned.1.call-done = bf16[1024,1024]{1,0:T(8,128)(2,1)} async-done(((bf16[16,1024]{1,0:T(8,128)(2,1)}), bf16[1024,1024]{1,0:T(8,128)(2,1)}) %all-gather.2.cloned.1.call-update) | async-done | bytes 2097168 | tf_op jit(solution)/shard_map/all_gather | solution.py:53
  98.1 1.7 fusion.34
  99.8 1.3 copy.93
  101.6 2.3 bitcast_reduce_fusion
  104.0 1.8 fusion.2
  105.8 3.1 fusion.7
  108.9 2.8 copy.72
  111.8 2.2 pad_maximum_fusion
  114.0 4.4 %all-to-all-start.1 = ((f32[8,2,128,258]{2,1,3,0:T(2,128)}), f32[8,2,128,258]{2,1,3,0:T(2,128)S(1)}, u32[]{:S(2)}, u32[]{:S(2)}) async-start(f32[8,2,128,258]{2,1,3,0:T(2,128)} %pad_maximum_fusion), calls=%async_computation.1 | async-start | bytes 4227072 | tf_op jit(solution)/shard_map/all_to_all | solution.py:60
  119.0 26.7 %all-to-all-done.1 = f32[8,2,128,258]{2,1,3,0:T(2,128)S(1)} async-done(((f32[8,2,128,258]{2,1,3,0:T(2,128)}), f32[8,2,128,258]{2,1,3,0:T(2,128)S(1)}, u32[]{:S(2)}, u32[]{:S(2)}) %all-to-all-start.1) | async-done | bytes 2113568 | tf_op jit(solution)/shard_map/all_to_all | solution.py:60
  145.8 1.0 fusion.9
  146.9 0.9 multiply_reduce_fusion.1
  148.1 12.8 %all_to_all.36 = bf16[8,1,128,256]{3,2,1,0:T(8,128)(2,1)S(1)} all-to-all(bf16[8,1,128,256]{3,2,1,0:T(8,128)(2,1)S(1)} %broadcast_in_dim.12), channel_id=1, replica_groups=mesh['sp'=64,'tp'=8] {'tp'}, dimensions={0} | all-to-all | bytes 1048576 | tf_op jit(solution)/shard_map/all_to_all | solution.py:33
  161.3 7.7 %all_to_all.37 = f32[8,1,128]{2,1,0:T(1,128)S(1)} all-to-all(f32[8,1,128]{2,1,0:T(1,128)S(1)} %broadcast_in_dim.13), channel_id=1, replica_groups=mesh['sp'=64,'tp'=8] {'tp'}, dimensions={0} | all-to-all | bytes 8192 | tf_op jit(solution)/shard_map/all_to_all | solution.py:33
  170.0 3.5 all-to-all-start.4
  173.6 10.2 %all-to-all-done.4 = bf16[8,128,256]{1,2,0:T(8,128)(2,1)S(1)} async-done(((bf16[8,128,256]{1,2,0:T(8,128)(2,1)}), bf16[8,128,256]{1,2,0:T(8,128)(2,1)S(1)}, u32[]{:S(2)}, u32[]{:S(2)}) %all-to-all-start.4) | async-done | bytes 524320 | tf_op jit(solution)/shard_map/all_to_all | solution.py:33
  183.8 1.1 stack.2
  184.8 210.2 %all_to_all.38 = bf16[64,32,2048]{2,1,0:T(8,128)(2,1)} all-to-all(bf16[64,32,2048]{2,1,0:T(8,128)(2,1)S(1)} %stack.2), channel_id=1, replica_groups=mesh['sp'=64,'tp'=8] {'sp'}, dimensions={0} | all-to-all | bytes 16777216 | tf_op jit(solution)/shard_map/all_to_all | solution.py:19
  395.0 5.6 %fusion.3 = f32[128,2048]{1,0:T(8,128)S(1)} fusion(bf16[2048,2048]{1,0:T(8,128)(2,1)} %bitcast.73, bf16[128,2048]{0,1:T(8,128)(2,1)S(1)} %bitcast.80), kind=kOutput, calls=%fused_computation.5 | convolution fusion | flops 1074135040 | bytes 9961472 | tf_op jit(solution)/shard_map/dot_general | solution.py:164
  400.7 18.4 %all_to_all.39 = f32[8,128,256]{2,1,0:T(8,128)S(1)} all-to-all(f32[8,128,256]{2,1,0:T(8,128)S(1)} %bitcast.74), channel_id=1, replica_groups=mesh['sp'=64,'tp'=8] {'tp'}, dimensions={0} | all-to-all | bytes 2097152 | tf_op jit(solution)/shard_map/all_to_all | solution.py:84
  (46 shorter events, 3.9 us)
Async XLA Ops:
  6.5 154.3 %copy-start = (bf16[2048,256]{1,0:T(8,128)(2,1)S(1)}, bf16[2048,256]{1,0:T(8,128)(2,1)}, u32[]{:S(2)}) copy-start(bf16[2048,256]{1,0:T(8,128)(2,1)} %param.16) | copy-start | bytes 3145732
  6.5 91.6 %all-gather.2.cloned.1.call-start = ((), (), s32[]{:S(2)}) async-start(), calls=%async_computation.7 | async-start | bytes 2129920 | tf_op jit(solution)/shard_map/all_gather | solution.py:53
  9.8 91.8 %all-to-all-start = ((bf16[8,128,256]{1,2,0:T(8,128)(2,1)}), bf16[8,128,256]{1,2,0:T(8,128)(2,1)}, u32[]{:S(2)}, u32[]{:S(2)}) async-start(bf16[8,128,256]{1,2,0:T(8,128)(2,1)} %broadcast_in_dim.10), calls=%async_computation | async-start | bytes 1048576 | tf_op jit(solution)/shard_map/all_to_all | solution.py:33
  104.0 1.8 copy-start.1
  111.8 6.6 %copy-start.7 = (f32[8]{0:T(128)S(1)}, f32[8]{0:T(128)}, u32[]{:S(2)}) copy-start(f32[8]{0:T(128)} %param.14) | copy-start | bytes 100
  114.0 33.8 %copy-start.5 = (f32[256]{0:T(256)S(1)}, f32[256]{0:T(256)}, u32[]{:S(2)}) copy-start(f32[256]{0:T(256)} %param.15) | copy-start | bytes 3076
  114.0 46.9 %copy-start.4 = (bf16[128,256]{1,0:T(8,128)(2,1)S(1)}, bf16[128,256]{1,0:T(8,128)(2,1)}, u32[]{:S(2)}) copy-start(bf16[128,256]{1,0:T(8,128)(2,1)} %param.10) | copy-start | bytes 196612
  114.0 31.7 %all-to-all-start.1 = ((f32[8,2,128,258]{2,1,3,0:T(2,128)}), f32[8,2,128,258]{2,1,3,0:T(2,128)S(1)}, u32[]{:S(2)}, u32[]{:S(2)}) async-start(f32[8,2,128,258]{2,1,3,0:T(2,128)} %pad_maximum_fusion), calls=%async_computation.1 | async-start | bytes 4227072 | tf_op jit(solution)/shard_map/all_to_all | solution.py:60
  118.4 50.6 %copy-start.6 = (f32[256]{0:T(256)S(1)}, f32[256]{0:T(256)}, u32[]{:S(2)}) copy-start(f32[256]{0:T(256)} %param.17) | copy-start | bytes 3076
  145.8 27.7 %copy-start.2 = (bf16[1024,32]{0,1:T(8,128)(2,1)S(1)}, bf16[1024,32]{0,1:T(8,128)(2,1)}, u32[]{:S(2)}) copy-start(bf16[1024,32]{0,1:T(8,128)(2,1)} %param.19) | copy-start | bytes 196612
  145.8 27.7 %copy-start.3 = (bf16[32,1024]{1,0:T(8,128)(2,1)S(1)}, bf16[32,1024]{1,0:T(8,128)(2,1)}, u32[]{:S(2)}) copy-start(bf16[32,1024]{1,0:T(8,128)(2,1)} %param.18) | copy-start | bytes 196612
  170.0 13.7 %all-to-all-start.4 = ((bf16[8,128,256]{1,2,0:T(8,128)(2,1)}), bf16[8,128,256]{1,2,0:T(8,128)(2,1)S(1)}, u32[]{:S(2)}, u32[]{:S(2)}) async-start(bf16[8,128,256]{1,2,0:T(8,128)(2,1)} %broadcast_in_dim.28), calls=%async_computation.4 | async-start | bytes 1048576 | tf_op jit(solution)/shard_map/all_to_all | solution.py:33
Sparse Core Ops, SparseCore 0:
  10.4 87.6 all-gather.1
